TPU v7x, 32 devices: a whole 2x2x4 slice. The times are simulated.
32 devices in a mesh: grp: 1, ep: 16 (over z, y, x), tp: 2 (over core).
Axes of the slice: x: 2, y: 2, z: 4, core: 2. Of those that a mesh axis runs over, the one named last changes fastest.
Arguments:
- tokens: bfloat16 [512, 2048], P(('grp', 'ep')), may hold values from -6 to 6
- in_gain: bfloat16 [2048], replicated, may hold values from 0.099609375 to 1.8984375
- route_expert: int32 [512, 6], P(('grp', 'ep')), may hold values from 0 to 15, all different within a row; in each aligned block of 32 rows (0 to 31, 32 to 63, ...) at most 16 rows name the same one
- route_weight: float32 [512, 6], P(('grp', 'ep')), may hold values from 0.05 to 1
- gate_weight: bfloat16 [16, 2048, 768], P('ep', None, 'tp'), may hold values from -0.125 to 0.125
- up_weight: bfloat16 [16, 2048, 768], P('ep', None, 'tp'), may hold values from -0.125 to 0.125
- down_weight: bfloat16 [16, 768, 2048], P('ep', 'tp'), may hold values from -1 to 1
- shared_gate: bfloat16 [2048, 768], P(None, 'tp'), may hold values from -0.125 to 0.125
- shared_up: bfloat16 [2048, 768], P(None, 'tp'), may hold values from -0.125 to 0.125
- shared_down: bfloat16 [768, 2048], P('tp'), may hold values from -1 to 1
- out_gain: bfloat16 [2048], P('tp'), may hold values from 0.099609375 to 1.8984375
Outputs:
- mixed: bfloat16 [512, 2048], P(('grp', 'ep'), 'tp')
Inputs may be any that keep to these rules, and one draw needn't show every extreme that they name: `route_expert`: each row names 6 different experts. Among the rows of one device no expert is named more than 16 times, a bound that some block reaches.
All inputs are finite; a program needn't handle non-finite values.
Results may differ from a plain program's by a relative error of at most 0.0077.
Values may be sent and summed in bfloat16 or wider, within the bound.
A program may use at most 64 MiB of HBM per device.

v0:
```python
import functools

import jax
import jax.numpy as jnp
from jax import lax
from jax.experimental import pallas as pl
from jax.experimental.pallas import tpu as pltpu
from jax.sharding import PartitionSpec as P

EPSILON = 1e-06
F32 = jnp.float32
BF16 = jnp.bfloat16


def dot(a, b):
    return jnp.dot(a, b, preferred_element_type=F32)


def dot_t(a, b):
    return lax.dot_general(a, b, (((1,), (1,)), ((), ())), preferred_element_type=F32)


def silu_product(gate_value, upward):
    return (gate_value * (1.0 / (1.0 + jnp.exp(-gate_value))) * upward).astype(BF16)


def kernel(
    outer,
    inner,
    cap,
    info_width,
    tokens_hbm,
    in_gain_hbm,
    route_expert_hbm,
    route_weight_hbm,
    out_gain_hbm,
    gate_hbm,
    up_hbm,
    down_hbm,
    sgate_hbm,
    sup_hbm,
    sdown_hbm,
    mixed,
    tokens,
    in_gain,
    route_expert,
    route_weight,
    out_gain,
    gate_w,
    up_w,
    down_w,
    sgate_w,
    sup_w,
    sdown_w,
    normed,
    column,
    staged,
    rows_in,
    part_out,
    part_in,
    part_own,
    result,
    back,
    sum_out,
    sum_in,
    shared_out,
    shared_in,
    squares_out,
    squares_in,
    w_sem,
    col_send,
    col_recv,
    col_pass,
    plane_send,
    plane_recv,
    pair_send,
    pair_recv,
    part_send,
    part_recv,
    shared_sem,
    back_send,
    back_recv,
    sum_send,
    sum_recv,
    sq_sem,
):
    ep = lax.axis_index("ep")
    tp = lax.axis_index("tp")
    z = ep // inner
    p = ep % inner
    other = 1 - tp
    experts = outer * inner
    local_tokens, width = tokens.shape
    half = width // 2

    loads = [
        pltpu.make_async_copy(src, dst, w_sem.at[i])
        for i, (src, dst) in enumerate(
            [
                (tokens_hbm, tokens),
                (in_gain_hbm, in_gain),
                (route_expert_hbm, route_expert),
                (route_weight_hbm, route_weight),
                (out_gain_hbm, out_gain),
                (sgate_hbm, sgate_w),
                (sup_hbm, sup_w),
                (sdown_hbm, sdown_w),
                (gate_hbm.at[0], gate_w),
                (up_hbm.at[0], up_w),
                (down_hbm.at[0], down_w),
            ]
        )
    ]
    for load in loads[:5]:
        load.start()

    barrier = pltpu.get_barrier_semaphore()

    def greet(ep_to, tp_to):
        pl.semaphore_signal(
            barrier, inc=1, device_id={"ep": ep_to, "tp": tp_to}, device_id_type=pl.DeviceIdType.MESH
        )

    for d in range(1, outer):
        greet(lax.rem(z + d, outer) * inner + p, tp)
    for d in range(1, inner):
        greet(z * inner + lax.rem(p + d, inner), tp)
    greet(ep, other)

    def remote(src, dst, send, recv, ep_to, tp_to):
        return pltpu.make_async_remote_copy(
            src_ref=src,
            dst_ref=dst,
            send_sem=send,
            recv_sem=recv,
            device_id={"ep": ep_to, "tp": tp_to},
            device_id_type=pl.DeviceIdType.MESH,
        )

    for load in loads[:5]:
        load.wait()
    for load in loads[5:]:
        load.start()
    floats = tokens[...].astype(F32)
    mean = jnp.sum(floats * floats, axis=1, keepdims=True) / width
    rows = (floats * lax.rsqrt(mean + EPSILON) * in_gain[...].astype(F32)[None, :]).astype(BF16)
    normed[...] = rows

    fact = lax.broadcasted_iota(jnp.int32, (info_width, local_tokens), 0)
    fact_expert = lax.rem(fact, experts)
    named = jnp.zeros((info_width, local_tokens), F32)
    weight = jnp.zeros((info_width, local_tokens), F32)
    for k in range(route_expert.shape[0]):
        hit = route_expert[k : k + 1, :] == fact_expert
        named = named + jnp.where(hit, 1.0, 0.0)
        weight = weight + jnp.where(hit, route_weight[k : k + 1, :], 0.0)
    row_i = lax.broadcasted_iota(jnp.int32, (local_tokens, local_tokens), 0)
    col_i = lax.broadcasted_iota(jnp.int32, (local_tokens, local_tokens), 1)
    upto = jnp.where(row_i <= col_i, 1.0, 0.0).astype(BF16)
    place = dot(named.astype(BF16), upto) * named
    high = weight.astype(BF16).astype(F32)
    facts = jnp.where(fact < experts, place, jnp.where(fact < 2 * experts, high, weight - high))
    facts = jnp.where(fact < 3 * experts, facts, 0.0).astype(BF16)
    same = jnp.where(row_i == col_i, 1.0, 0.0).astype(BF16)
    info = dot_t(same, facts)

    @pl.when(tp == 0)
    def _():
        column[z, :, :half] = rows[:, :half]

    @pl.when(tp == 1)
    def _():
        column[z, :, :half] = rows[:, half:]

    column[z, :, half:] = info.astype(BF16)

    pl.semaphore_wait(barrier, outer + inner - 1)

    sends = []

    def send(src, dst, send_sem, recv_sem, ep_to, tp_to):
        copy = remote(src, dst, send_sem, recv_sem, ep_to, tp_to)
        copy.start()
        sends.append(copy)

    def arrive(ref, send_sem, recv_sem):
        remote(ref, ref, send_sem, recv_sem, ep, other).wait_recv()

    short = jnp.minimum(z, outer - 1 - z)

    def nth(i):
        if i == 0:
            return z
        near = (i + 1) // 2 if i % 2 else -(i // 2)
        far = jnp.where(z < outer - 1 - z, i - short, short - i)
        return z + jnp.where(i <= 2 * short, near, far)

    order = [nth(i) for i in range(outer)]

    def column_copy(block, to, send_sem):
        here = column.at[block]
        return remote(here, here, send_sem, col_recv.at[block], to * inner + p, tp)

    def direct(to):
        return (to - z) * (to - z) != 4

    def passes(j):
        on = 2 * z - j
        return on, ((j - z) * (j - z) == 1) & (on >= 0) & (on < outer)

    for to in order[1:]:

        @pl.when(direct(to))
        def _(to=to):
            column_copy(z, to, col_send.at[to]).start()


    slots = inner * cap
    slot_row = lax.broadcasted_iota(jnp.int32, (slots, info_width), 0)
    slot_lane = lax.broadcasted_iota(jnp.int32, (slots, info_width), 1)
    slot_expert = z * inner + slot_row // cap

    def selector(offset):
        return jnp.where(slot_lane == slot_expert + offset, 1.0, 0.0).astype(BF16)

    pick_place = selector(0)
    pick_high = selector(experts)
    pick_low = selector(2 * experts)
    slot_rank = (lax.broadcasted_iota(jnp.int32, (slots, local_tokens), 0) % cap + 1).astype(F32)
    slot_of_lane = (lax.broadcasted_iota(jnp.int32, (local_tokens, slots), 1) % cap + 1).astype(F32)
    peers = [lax.rem(p + e, inner) for e in range(1, inner)]

    def half_of(which):
        return pl.ds(pl.multiple_of(which * half, half), half)

    def dispatch(i):
        j = order[i]
        if i:
            arrive(column.at[j], col_send.at[j], col_recv.at[j])
            on, wanted = passes(j)

            @pl.when(wanted)
            def _():
                column_copy(j, on, col_pass.at[j]).start()

        where = dot_t(pick_place, column[j, :, half:])
        onehot = jnp.where(where == slot_rank, 1.0, 0.0).astype(BF16)
        moved = dot(onehot, column[j, :, :half]).astype(BF16)
        staged[j] = moved.reshape(inner, cap, half)
        for to in peers:
            send(
                staged.at[j, to],
                rows_in.at[tp, j, p],
                plane_send.at[j, to],
                plane_recv.at[j, p],
                z * inner + to,
                tp,
            )
        rows_in[tp, j, p] = staged[j, p]

    def pair(i):
        j = order[i]
        for source in peers:
            arrive(rows_in.at[tp, j, source], plane_send.at[j, source], plane_recv.at[j, source])
        here = rows_in.at[tp, j]
        send(here, here, pair_send.at[j], pair_recv.at[j], ep, other)

    def expert(group):
        if group[0] == 0:
            for load in loads[8:]:
                load.wait()

        def rows_of(which):
            blocks = [rows_in[which, order[i]].reshape(slots, half) for i in group]
            return jnp.concatenate(blocks, axis=0)

        own_rows = rows_of(tp)
        gate_value = dot(own_rows, gate_w[half_of(tp), :])
        upward = dot(own_rows, up_w[half_of(tp), :])
        for i in group:
            j = order[i]
            arrive(rows_in.at[other, j], pair_send.at[j], pair_recv.at[j])
        other_rows = rows_of(other)
        gate_value = gate_value + dot(other_rows, gate_w[half_of(other), :])
        upward = upward + dot(other_rows, up_w[half_of(other), :])
        hidden = silu_product(gate_value, upward)

        def store(target, values):
            for n, i in enumerate(group):
                block = values[n * slots : (n + 1) * slots]
                target[order[i]] = block.astype(BF16).reshape(inner, cap, half)

        store(part_out, dot(hidden, down_w[:, half_of(other)]))
        for i in reversed(group):
            j = order[i]
            send(part_out.at[j], part_in.at[j], part_send.at[j], part_recv.at[j], ep, other)
        store(part_own, dot(hidden, down_w[:, half_of(tp)]))

    def give_back(i):
        j = order[i]
        arrive(part_in.at[j], part_send.at[j], part_recv.at[j])
        result[j] = (part_own[j].astype(F32) + part_in[j].astype(F32)).astype(BF16)
        for to in peers:
            send(
                result.at[j, to],
                back.at[j, p],
                back_send.at[j, to],
                back_recv.at[j, p],
                z * inner + to,
                tp,
            )
        back[j, p] = result[j, p]

    def combine(i):
        j = order[i]
        facts = column[j, :, half:]
        chosen = dot_t(facts, pick_place) == slot_of_lane
        high_part = jnp.where(chosen, dot_t(facts, pick_high), 0.0).astype(BF16)
        low_part = jnp.where(chosen, dot_t(facts, pick_low), 0.0).astype(BF16)
        for source in peers:
            arrive(back.at[j, source], back_send.at[j, source], back_recv.at[j, source])
        values = back[j].reshape(slots, half)
        return dot(high_part, values) + dot(low_part, values)

    dispatch(0)

    for load in loads[5:8]:
        load.wait()
    inputs = normed[...]
    shared_hidden = silu_product(dot(inputs, sgate_w[...]), dot(inputs, sup_w[...]))
    shared_out[...] = dot(shared_hidden, sdown_w[:, half_of(other)]).astype(BF16)
    send(shared_out, shared_in, shared_sem.at[0], shared_sem.at[1], ep, other)
    shared_own = dot(shared_hidden, sdown_w[:, half_of(tp)]).astype(BF16)

    def step(task, what):
        with jax.named_scope(task.__name__ + str(what)):
            task(what)

    for i in range(1, outer):
        step(dispatch, i)
        if i == 1:
            step(pair, 0)
    step(pair, 1)
    for first in range(0, outer, 2):
        step(expert, (first, first + 1))
        if first + 2 < outer:
            step(pair, first + 2)
            step(pair, first + 3)
        step(give_back, first + 1)
        step(give_back, first)

    for i in [1] + list(range(outer - 1, 1, -1)):
        j = order[i]
        with jax.named_scope("combine" + str(i)):
            sum_out[j] = combine(i).astype(BF16)
            send(sum_out.at[j], sum_in.at[z], sum_send.at[j], sum_recv.at[z], j * inner + p, tp)
    with jax.named_scope("combine0"):
        combined = combine(0)
        arrive(shared_in, shared_sem.at[0], shared_sem.at[1])
        shared_rows = (shared_own.astype(F32) + shared_in[...].astype(F32)).astype(BF16)
        combined = combined + shared_rows.astype(F32)
    for j in order[1:]:
        arrive(sum_in.at[j], sum_send.at[j], sum_recv.at[j])
        combined = combined + sum_in[j].astype(F32)

    own_squares = jnp.sum(combined * combined, axis=1, keepdims=True)
    squares_out[...] = jnp.broadcast_to(own_squares, squares_out.shape)
    sq_copy = remote(squares_out, squares_in, sq_sem.at[0], sq_sem.at[1], ep, other)
    sq_copy.start()
    sq_copy.wait_recv()
    squares = own_squares + squares_in[:, :1]
    scaled = combined * lax.rsqrt(squares / width + EPSILON)
    mixed[...] = (scaled * out_gain[...].astype(F32)[None, :]).astype(BF16)

    for to in order[1:]:

        @pl.when(direct(to))
        def _(to=to):
            column_copy(z, to, col_send.at[to]).wait_send()

        on, wanted = passes(to)

        @pl.when(wanted)
        def _(to=to, on=on):
            column_copy(to, on, col_pass.at[to]).wait_send()

    for copy in sends:
        copy.wait_send()
    sq_copy.wait_send()


def body(
    experts,
    tokens,
    in_gain,
    route_expert,
    route_weight,
    gate_weight,
    up_weight,
    down_weight,
    shared_gate,
    shared_up,
    shared_down,
    out_gain,
):
    inner = 1
    while inner * inner < experts:
        inner *= 2
    outer = experts // inner
    local_tokens, width = tokens.shape
    half = width // 2
    top_count = route_expert.shape[1]
    capacity = max(2, (local_tokens * top_count * 4 + 3 * experts - 1) // (3 * experts))
    cap = -(-capacity // 16) * 16
    info_width = -(-3 * experts // 128) * 128
    hidden = gate_weight.shape[2]
    shared_width = shared_gate.shape[1]

    def vm(shape, kind=BF16):
        return pltpu.VMEM(shape, kind)

    grid_rows = (outer, inner, cap, half)
    dma = pltpu.SemaphoreType.DMA
    in_vmem = pl.BlockSpec(memory_space=pltpu.VMEM)
    anywhere = pl.BlockSpec(memory_space=pl.ANY)
    return pl.pallas_call(
        functools.partial(kernel, outer, inner, cap, info_width),
        out_shape=jax.ShapeDtypeStruct((local_tokens, half), BF16),
        in_specs=[anywhere] * 11,
        out_specs=in_vmem,
        scratch_shapes=[
            vm((local_tokens, width)),
            vm((width,)),
            vm((top_count, local_tokens), jnp.int32),
            vm((top_count, local_tokens), F32),
            vm((half,)),
            vm((width, hidden)),
            vm((width, hidden)),
            vm((hidden, width)),
            vm((width, shared_width)),
            vm((width, shared_width)),
            vm((shared_width, width)),
            vm((local_tokens, width)),
            vm((outer, local_tokens, half + info_width)),
            vm(grid_rows),
            vm((2,) + grid_rows),
            vm(grid_rows),
            vm(grid_rows),
            vm(grid_rows),
            vm(grid_rows),
            vm(grid_rows),
            vm((outer, local_tokens, half)),
            vm((outer, local_tokens, half)),
            vm((local_tokens, half)),
            vm((local_tokens, half)),
            vm((local_tokens, 128), F32),
            vm((local_tokens, 128), F32),
            dma((11,)),
            dma((outer,)),
            dma((outer,)),
            dma((outer,)),
            dma((outer, inner)),
            dma((outer, inner)),
            dma((outer,)),
            dma((outer,)),
            dma((outer,)),
            dma((outer,)),
            dma((2,)),
            dma((outer, inner)),
            dma((outer, inner)),
            dma((outer,)),
            dma((outer,)),
            dma((2,)),
        ],
        compiler_params=pltpu.CompilerParams(
            collective_id=0, has_side_effects=True, vmem_limit_bytes=60 * 1024 * 1024
        ),
    )(
        tokens,
        in_gain,
        route_expert.T,
        route_weight.T,
        out_gain,
        gate_weight,
        up_weight,
        down_weight,
        shared_gate,
        shared_up,
        shared_down,
    )


def solution(mesh):
    return jax.shard_map(
        functools.partial(body, mesh.shape["ep"]),
        mesh=mesh,
        in_specs=(
            P(("grp", "ep"), None),
            P(),
            P(("grp", "ep"), None),
            P(("grp", "ep"), None),
            P("ep", None, "tp"),
            P("ep", None, "tp"),
            P("ep", "tp", None),
            P(None, "tp"),
            P(None, "tp"),
            P("tp", None),
            P("tp"),
        ),
        out_specs=P(("grp", "ep"), "tp"),
        check_vma=False,
    )
```

profile of v0, /device:TPU:0, one launch (start us, length us, event | category | flops | bytes accessed | tf_op | source)
XLA Modules:
  0.0 33.8 jit_solution(2327113619095275704)
XLA Ops:
  0.0 32.3 %shard_map.109 = bf16[32,1024]{1,0:T(8,128)(2,1)} custom-call(bf16[32,2048]{1,0:T(8,128)(2,1)} %tokens_hbm.1, bf16[2048]{0:T(1024)(128)(2,1)} %in_gain_hbm.1, s32[6,32]{1,0:T(8,128)} %bitcast.2, f32[6,32]{1,0:T(8,128)} %bitcast.3, bf16[1024]{0:T(1024)(128)(2,1)} %out_gain_hbm.1, bf16[1,2048,384]{2,1,0:T(8,128)(2,1)} %gate_hbm.1, ...), custom_call_target="tpu_custom_call" | custom-call | tf_op jit(solution)/shard_map/pallas_call | solution.py:426
  32.3 1.5 %copy.13 = bf16[32,1024]{1,0:T(8,128)(2,1)} copy(bf16[32,1024]{1,0:T(8,128)(2,1)} %shard_map.109) | data formatting | bytes 131072
where the time goes:
time: 34 us; the launch traced here: 33.8 us
  Pallas kernels  32.3 us (95%)
  local copies, waits for them, and re-layouts  1.47 us (4%)
    pallas_call x1, Pallas kernels, body(): pl.pallas_call(functools.partial(kernel, outer, inner, cap, info_width),...  32.3 us
    unnamed x1, local copies, waits for them, and re-layouts  1.47 us

commit v1 on v0

v1 whole, which is shorter than its diff:
```python
import functools

import jax
import jax.numpy as jnp
from jax import lax
from jax.experimental import pallas as pl
from jax.experimental.pallas import tpu as pltpu
from jax.sharding import PartitionSpec as P

EPSILON = 1e-06
F32 = jnp.float32
BF16 = jnp.bfloat16


def dot(a, b):
    return jnp.dot(a, b, preferred_element_type=F32)


def dot_t(a, b):
    return lax.dot_general(a, b, (((1,), (1,)), ((), ())), preferred_element_type=F32)


def silu_product(gate_value, upward):
    return (gate_value * (1.0 / (1.0 + jnp.exp(-gate_value))) * upward).astype(BF16)


def kernel(
    outer,
    inner,
    cap,
    info_width,
    split,
    relay,
    tokens_hbm,
    in_gain_hbm,
    route_expert_hbm,
    route_weight_hbm,
    out_gain_hbm,
    gate_hbm,
    up_hbm,
    down_hbm,
    sgate_hbm,
    sup_hbm,
    sdown_hbm,
    mixed,
    tokens,
    in_gain,
    route_expert,
    route_weight,
    out_gain,
    gate_w,
    up_w,
    down_w,
    sgate_w,
    sup_w,
    sdown_w,
    normed,
    column,
    staged,
    rows_in,
    part_out,
    part_in,
    part_own,
    result,
    back,
    sum_out,
    sum_in,
    shared_out,
    shared_in,
    last_out,
    last_in,
    w_sem,
    col_send,
    col_recv,
    col_pass,
    plane_recv,
    pair_recv,
    part_recv,
    back_recv,
    sum_recv,
    send_sem,
    core_sem,
):
    ep = lax.axis_index("ep")
    tp = lax.axis_index("tp")
    z = ep // inner
    p = ep % inner
    experts = outer * inner
    local_tokens, width = tokens.shape
    half = width // 2

    loads = [
        pltpu.make_async_copy(src, dst, w_sem.at[i])
        for i, (src, dst) in enumerate(
            [
                (tokens_hbm, tokens),
                (in_gain_hbm, in_gain),
                (route_expert_hbm, route_expert),
                (route_weight_hbm, route_weight),
                (out_gain_hbm, out_gain),
                (sgate_hbm, sgate_w),
                (sup_hbm, sup_w),
                (sdown_hbm, sdown_w),
                (gate_hbm.at[0], gate_w),
                (up_hbm.at[0], up_w),
                (down_hbm.at[0], down_w),
            ]
        )
    ]
    for load in loads[:5]:
        load.start()

    barrier = pltpu.get_barrier_semaphore()

    def greet(ep_to, tp_to):
        pl.semaphore_signal(
            barrier, inc=1, device_id={"ep": ep_to, "tp": tp_to}, device_id_type=pl.DeviceIdType.MESH
        )

    for d in range(1, outer):
        greet(lax.rem(z + d, outer) * inner + p, tp)
    for d in range(1, inner):
        greet(z * inner + lax.rem(p + d, inner), tp)
    greet(ep, 1 - tp)

    for load in loads[:5]:
        load.wait()
    for load in loads[5:]:
        load.start()
    floats = tokens[...].astype(F32)
    mean = jnp.sum(floats * floats, axis=1, keepdims=True) / width
    rows = (floats * lax.rsqrt(mean + EPSILON) * in_gain[...].astype(F32)[None, :]).astype(BF16)
    normed[...] = rows

    fact = lax.broadcasted_iota(jnp.int32, (info_width, local_tokens), 0)
    fact_expert = lax.rem(fact, experts)
    named = jnp.zeros((info_width, local_tokens), F32)
    weight = jnp.zeros((info_width, local_tokens), F32)
    for k in range(route_expert.shape[0]):
        hit = route_expert[k : k + 1, :] == fact_expert
        named = named + jnp.where(hit, 1.0, 0.0)
        weight = weight + jnp.where(hit, route_weight[k : k + 1, :], 0.0)
    row_i = lax.broadcasted_iota(jnp.int32, (local_tokens, local_tokens), 0)
    col_i = lax.broadcasted_iota(jnp.int32, (local_tokens, local_tokens), 1)
    upto = jnp.where(row_i <= col_i, 1.0, 0.0).astype(BF16)
    place = dot(named.astype(BF16), upto) * named
    high = weight.astype(BF16).astype(F32)
    facts = jnp.where(fact < experts, place, jnp.where(fact < 2 * experts, high, weight - high))
    facts = jnp.where(fact < 3 * experts, facts, 0.0).astype(BF16)
    same = jnp.where(row_i == col_i, 1.0, 0.0).astype(BF16)
    info = dot_t(same, facts).astype(BF16)

    short = jnp.minimum(z, outer - 1 - z)

    def nth(i):
        if i == 0:
            return z
        near = (i + 1) // 2 if i % 2 else -(i // 2)
        far = jnp.where(z < outer - 1 - z, i - short, short - i)
        return z + jnp.where(i <= 2 * short, near, far)

    order = [nth(i) for i in range(outer)]

    def direct(to):
        if not relay:
            return z >= 0
        return (to - z) * (to - z) != 4

    def passes(j):
        on = 2 * z - j
        return on, ((j - z) * (j - z) == 1) & (on >= 0) & (on < outer)

    slots = inner * cap
    slot_row = lax.broadcasted_iota(jnp.int32, (slots, info_width), 0)
    slot_lane = lax.broadcasted_iota(jnp.int32, (slots, info_width), 1)
    slot_expert = z * inner + slot_row // cap

    def selector(offset):
        return jnp.where(slot_lane == slot_expert + offset, 1.0, 0.0).astype(BF16)

    slot_rank = (lax.broadcasted_iota(jnp.int32, (slots, local_tokens), 0) % cap + 1).astype(F32)
    slot_of_lane = (lax.broadcasted_iota(jnp.int32, (local_tokens, slots), 1) % cap + 1).astype(F32)
    peers = [lax.rem(p + e, inner) for e in range(1, inner)]

    pl.semaphore_wait(barrier, outer + inner - 1)

    def on_core(core):
        edges = (0, split, width)
        first, end = edges[core], edges[core + 1]
        count = end - first
        other = 1 - core
        mine = pl.ds(first, count)
        theirs = pl.ds(edges[other], edges[other + 1] - edges[other])
        facts_at = pl.ds(first, info_width)
        rows_at = pl.ds(first + info_width, count)
        sent_at = pl.ds(first, info_width + count)

        def pieces(which):
            begin, stop = edges[which], edges[which + 1]
            parts = PIECES[which] if (stop - begin) % (128 * PIECES[which]) == 0 else 1
            size = (stop - begin) // parts
            return [pl.ds(begin + n * size, size) for n in range(parts)]

        my_pieces = pieces(core)

        column[z, :, facts_at] = info
        column[z, :, rows_at] = rows[:, first:end]

        def remote(src, dst, send, recv, ep_to, tp_to):
            return pltpu.make_async_remote_copy(
                src_ref=src,
                dst_ref=dst,
                send_sem=send,
                recv_sem=recv,
                device_id={"ep": ep_to, "tp": tp_to},
                device_id_type=pl.DeviceIdType.MESH,
            )

        def send(src, dst, kind, recv_sem, ep_to, tp_to):
            remote(src, dst, send_sem.at[kind], recv_sem, ep_to, tp_to).start()

        def arrive(ref, recv_sem):
            with jax.named_scope("w"):
                remote(ref, ref, send_sem.at[0], recv_sem, ep, other).wait_recv()

        def sent(ref, kind):
            remote(ref, ref, send_sem.at[kind], col_recv.at[0], ep, other).wait_send()

        def column_copy(block, to, sem):
            here = column.at[block, :, sent_at]
            return remote(here, here, sem, col_recv.at[block], to * inner + p, core)

        for to in order[1:]:

            @pl.when(direct(to))
            def _(to=to):
                column_copy(z, to, col_send.at[to]).start()

        pick_place = selector(0)
        pick_high = selector(experts)
        pick_low = selector(2 * experts)

        def dispatch(i):
            j = order[i]
            if i:
                arrive(column.at[j, :, sent_at], col_recv.at[j])
                if relay:
                    on, wanted = passes(j)

                    @pl.when(wanted)
                    def _():
                        column_copy(j, on, col_pass.at[j]).start()

            where = dot_t(pick_place, column[j, :, facts_at])
            onehot = jnp.where(where == slot_rank, 1.0, 0.0).astype(BF16)
            moved = dot(onehot, column[j, :, rows_at]).astype(BF16)
            staged[j, :, :, mine] = moved.reshape(inner, cap, count)
            for to in peers:
                send(
                    staged.at[j, to, :, mine],
                    rows_in.at[j, p, :, mine],
                    0,
                    plane_recv.at[j],
                    z * inner + to,
                    core,
                )
            rows_in[j, p, :, mine] = staged[j, p, :, mine]

        def pair(i):
            j = order[i]
            arrive(rows_in.at[j, pl.ds(0, inner - 1), :, mine], plane_recv.at[j])
            here = rows_in.at[j, :, :, mine]
            send(here, here, 1, pair_recv.at[j], ep, other)

        def expert(*group):
            if group[0] == 0:
                for load in loads[8:]:
                    load.wait()

            def rows_of(columns):
                blocks = [rows_in[order[i], :, :, columns].reshape(slots, columns.size) for i in group]
                return blocks[0] if len(blocks) == 1 else jnp.concatenate(blocks, axis=0)

            own_rows = rows_of(mine)
            gate_value = dot(own_rows, gate_w[mine, :])
            upward = dot(own_rows, up_w[mine, :])
            for i in group:
                j = order[i]
                arrive(rows_in.at[j, :, :, theirs], pair_recv.at[j])
            other_rows = rows_of(theirs)
            gate_value = gate_value + dot(other_rows, gate_w[theirs, :])
            upward = upward + dot(other_rows, up_w[theirs, :])
            hidden = silu_product(gate_value, upward)

            def store(target, columns):
                values = dot(hidden, down_w[:, columns]).astype(BF16)
                for n, i in enumerate(group):
                    block = values[n * slots : (n + 1) * slots]
                    target[order[i], :, :, columns] = block.reshape(inner, cap, columns.size)

            for n, piece in enumerate(pieces(other)):
                store(part_out, piece)
                for i in reversed(group):
                    j = order[i]
                    here = part_out.at[j, :, :, piece]
                    send(here, part_in.at[j, :, :, piece], 2, part_recv.at[j, n], ep, other)
            for piece in my_pieces:
                store(part_own, piece)

        def give_back(i):
            j = order[i]
            for n, piece in enumerate(my_pieces):
                arrive(part_in.at[j, :, :, piece], part_recv.at[j, n])
                total = part_own[j, :, :, piece].astype(F32) + part_in[j, :, :, piece].astype(F32)
                result[j, :, :, piece] = total.astype(BF16)
                for to in peers:
                    send(
                        result.at[j, to, :, piece],
                        back.at[j, p, :, piece],
                        3,
                        back_recv.at[j, n],
                        z * inner + to,
                        core,
                    )
                back[j, p, :, piece] = result[j, p, :, piece]

        def weigh(i):
            known = column[order[i], :, facts_at]
            chosen = dot_t(known, pick_place) == slot_of_lane
            high_part = jnp.where(chosen, dot_t(known, pick_high), 0.0).astype(BF16)
            low_part = jnp.where(chosen, dot_t(known, pick_low), 0.0).astype(BF16)
            return high_part, low_part

        def gathered(i, weights, n, piece):
            j = order[i]
            arrive(back.at[j, pl.ds(0, inner - 1), :, piece], back_recv.at[j, n])
            values = back[j, :, :, piece].reshape(slots, piece.size)
            return dot(weights[0], values) + dot(weights[1], values)

        def combine(i):
            j = order[i]
            weights = weigh(i)
            for n, piece in enumerate(my_pieces):
                sum_out[i - 1, :, piece] = gathered(i, weights, n, piece).astype(BF16)
                here = sum_out.at[i - 1, :, piece]
                send(here, sum_in.at[z, :, piece], 4, sum_recv.at[z, n], j * inner + p, core)

        def shared():
            for load in loads[5:8]:
                load.wait()
            inputs = normed[...]
            hidden = silu_product(dot(inputs, sgate_w[...]), dot(inputs, sup_w[...]))
            shared_out[:, theirs] = dot(hidden, sdown_w[:, theirs]).astype(BF16)
            here = shared_out.at[:, theirs]
            send(here, shared_in.at[:, theirs], 5, core_sem.at[0], ep, other)
            shared_out[:, mine] = dot(hidden, sdown_w[:, mine]).astype(BF16)

        def step(task, *what):
            with jax.named_scope(task.__name__ + "".join(str(w) for w in what)):
                task(*what)

        for task, *what in PLAN(outer, dispatch, shared, pair, expert, give_back, combine):
            step(task, *what)

        totals = []
        with jax.named_scope("own"):
            weights = weigh(0)
            arrive(shared_in.at[:, mine], core_sem.at[0])
            for n, piece in enumerate(my_pieces):
                shared_rows = shared_out[:, piece].astype(F32) + shared_in[:, piece].astype(F32)
                totals.append(gathered(0, weights, n, piece) + shared_rows.astype(BF16).astype(F32))
        with jax.named_scope("sums"):
            for i in range(1, outer):
                j = order[i]
                for n, piece in enumerate(my_pieces):
                    arrive(sum_in.at[j, :, piece], sum_recv.at[j, n])
                    totals[n] = totals[n] + sum_in[j, :, piece].astype(F32)
        combined = totals[0] if len(totals) == 1 else jnp.concatenate(totals, axis=1)

        lanes = last_out.shape[1] - (half - split)
        squares_at = pl.ds(half - split, lanes)
        own_squares = jnp.sum(combined * combined, axis=1, keepdims=True)
        last_out[:, squares_at] = jnp.broadcast_to(own_squares, (local_tokens, lanes))
        if core == 0:
            leaving, coming = squares_at, pl.ds(0, half - split + lanes)
        else:
            leaving, coming = pl.ds(0, half - split + lanes), squares_at
            if half > split:
                last_out[:, : half - split] = combined[:, : half - split]
        here = last_out.at[:, leaving]
        send(here, last_in.at[:, leaving], 6, core_sem.at[1], ep, other)
        with jax.named_scope("lastwait"):
            arrive(last_in.at[:, coming], core_sem.at[1])
        squares = own_squares + last_in[:, half - split : half - split + 1]
        scale = lax.rsqrt(squares / width + EPSILON)
        gain = out_gain[...].astype(F32)[None, :]
        if core == 0:
            mixed[:, :split] = (combined * scale * gain[:, :split]).astype(BF16)
            if half > split:
                extra = last_in[:, : half - split] * scale * gain[:, split:]
                mixed[:, split:] = extra.astype(BF16)
        else:
            mixed[...] = (combined[:, half - split :] * scale * gain).astype(BF16)

        for to in order[1:]:

            @pl.when(direct(to))
            def _(to=to):
                column_copy(z, to, col_send.at[to]).wait_send()

            if relay:
                on, wanted = passes(to)

                @pl.when(wanted)
                def _(to=to, on=on):
                    column_copy(to, on, col_pass.at[to]).wait_send()

        sent(staged.at[:, pl.ds(0, inner - 1), :, mine], 0)
        sent(rows_in.at[:, :, :, mine], 1)
        sent(part_out.at[:, :, :, theirs], 2)
        sent(result.at[:, pl.ds(0, inner - 1), :, mine], 3)
        sent(sum_out.at[:, :, mine], 4)
        sent(shared_out.at[:, theirs], 5)
        sent(here, 6)

    for core in range(2):

        @pl.when(tp == core)
        def _(core=core):
            on_core(core)


def plan(outer, dispatch, shared, pair, expert, give_back, combine):
    steps = [(dispatch, 0), (shared,), (dispatch, 1)]
    for i in range(2, outer):
        steps += [(dispatch, i), (pair, i - 2)]
    steps += [(pair, outer - 2), (expert, 0, 1)]
    for i in range(2, outer):
        steps += [(give_back, 1), (give_back, 0)] if i == 2 else [(give_back, i - 1)]
        steps += [(pair, outer - 1)] if i == outer - 1 else []
        steps += [(expert, i)]
    steps += [(give_back, outer - 1)]
    steps += [(combine, i) for i in range(1, outer)]
    return steps


PLAN = plan
PIECES = (1, 2)
SPLIT = 4
RELAY = True


def body(
    experts,
    tokens,
    in_gain,
    route_expert,
    route_weight,
    gate_weight,
    up_weight,
    down_weight,
    shared_gate,
    shared_up,
    shared_down,
    out_gain,
):
    inner = 1
    while inner * inner < experts:
        inner *= 2
    outer = experts // inner
    local_tokens, width = tokens.shape
    half = width // 2
    split = width * SPLIT // 16
    top_count = route_expert.shape[1]
    capacity = max(2, (local_tokens * top_count * 4 + 3 * experts - 1) // (3 * experts))
    cap = -(-capacity // 16) * 16
    info_width = -(-3 * experts // 128) * 128
    hidden = gate_weight.shape[2]
    shared_width = shared_gate.shape[1]

    def vm(shape, kind=BF16):
        return pltpu.VMEM(shape, kind)

    grid_rows = (outer, inner, cap, width)
    most = max(PIECES)
    dma = pltpu.SemaphoreType.DMA
    in_vmem = pl.BlockSpec(memory_space=pltpu.VMEM)
    in_hbm = pl.BlockSpec(memory_space=pltpu.HBM)
    return pl.pallas_call(
        functools.partial(kernel, outer, inner, cap, info_width, split, RELAY),
        out_shape=pltpu.VMEM((local_tokens, half), BF16),
        in_specs=[in_hbm] * 11,
        out_specs=in_vmem,
        scratch_shapes=[
            vm((local_tokens, width)),
            vm((width,)),
            vm((top_count, local_tokens), jnp.int32),
            vm((top_count, local_tokens), F32),
            vm((half,)),
            vm((width, hidden)),
            vm((width, hidden)),
            vm((hidden, width)),
            vm((width, shared_width)),
            vm((width, shared_width)),
            vm((shared_width, width)),
            vm((local_tokens, width)),
            vm((outer, local_tokens, width + info_width)),
            vm(grid_rows),
            vm(grid_rows),
            vm(grid_rows),
            vm(grid_rows),
            vm(grid_rows),
            vm(grid_rows),
            vm(grid_rows),
            vm((outer - 1, local_tokens, width)),
            vm((outer, local_tokens, width)),
            vm((local_tokens, width)),
            vm((local_tokens, width)),
            vm((local_tokens, half - split + 128), F32),
            vm((local_tokens, half - split + 128), F32),
            dma((11,)),
            dma((outer,)),
            dma((outer,)),
            dma((outer,)),
            dma((outer,)),
            dma((outer,)),
            dma((outer, most)),
            dma((outer, most)),
            dma((outer, most)),
            dma((7,)),
            dma((2,)),
        ],
        compiler_params=pltpu.CompilerParams(
            collective_id=0, has_side_effects=True, vmem_limit_bytes=60 * 1024 * 1024
        ),
    )(
        tokens,
        in_gain,
        route_expert.T,
        route_weight.T,
        out_gain,
        gate_weight,
        up_weight,
        down_weight,
        shared_gate,
        shared_up,
        shared_down,
    )


def solution(mesh):
    return jax.shard_map(
        functools.partial(body, mesh.shape["ep"]),
        mesh=mesh,
        in_specs=(
            P(("grp", "ep"), None),
            P(),
            P(("grp", "ep"), None),
            P(("grp", "ep"), None),
            P("ep", None, "tp"),
            P("ep", None, "tp"),
            P("ep", "tp", None),
            P(None, "tp"),
            P(None, "tp"),
            P("tp", None),
            P("tp"),
        ),
        out_specs=P(("grp", "ep"), "tp"),
        check_vma=False,
    )
```

time: 34 us -> 33.9 us (level)
  local copies, waits for them, and re-layouts: 1.47 us -> 0.63 us
  Pallas kernels: 32.3 us -> 33.1 us
    unnamed x1, local copies, waits for them, and re-layouts: 1.47 us -> 0.63 us
    pallas_call x1, Pallas kernels: 32.3 us -> 33.1 us  [body(): pl.pallas_call(functools.partial(kernel, outer, inner, cap, info_width, s...]
where the time goes in v1:
time: 33.9 us; the launch traced here: 33.7 us
  Pallas kernels  33.1 us (98%)
  local copies, waits for them, and re-layouts  0.63 us (2%)
    pallas_call x1, Pallas kernels, body(): pl.pallas_call(functools.partial(kernel, outer, inner, cap, info_width, s...  33.1 us

profile of v1, /device:TPU:0, one launch (start us, length us, event | category | flops | bytes accessed | tf_op | source)
XLA Modules:
  0.0 33.7 jit_solution(14963550826661570731)
XLA Ops:
  0.0 33.1 %shard_map.109 = bf16[32,1024]{1,0:T(8,128)(2,1)S(1)} custom-call(bf16[32,2048]{1,0:T(8,128)(2,1)} %tokens_hbm.1, bf16[2048]{0:T(1024)(128)(2,1)} %in_gain_hbm.1, s32[6,32]{1,0:T(8,128)} %bitcast.2, f32[6,32]{1,0:T(8,128)} %bitcast.3, bf16[1024]{0:T(1024)(128)(2,1)} %out_gain_hbm.1, bf16[1,2048,384]{2,1,0:T(8,128)(2,1)} %gate_hbm.1, ...), custom_call_target="tpu_custom_call" | custom-call | tf_op jit(solution)/shard_map/pallas_call | solution.py:489
  33.1 0.6 %copy.13 = bf16[32,1024]{1,0:T(8,128)(2,1)} copy(bf16[32,1024]{1,0:T(8,128)(2,1)S(1)} %shard_map.109) | data formatting | bytes 131072

commit v2 on v1

--- a/solution.py
+++ b/solution.py
@@ -157,6 +157,9 @@
             return z
         near = (i + 1) // 2 if i % 2 else -(i // 2)
         far = jnp.where(z < outer - 1 - z, i - short, short - i)
+        if i > 1:
+            ends = i + 1 if i < outer - 1 else 2
+            far = jnp.where(short > 0, far, jnp.where(z == 0, ends, -ends))
         return z + jnp.where(i <= 2 * short, near, far)
 
     order = [nth(i) for i in range(outer)]
@@ -433,14 +436,15 @@
 def plan(outer, dispatch, shared, pair, expert, give_back, combine):
     steps = [(dispatch, 0), (shared,), (dispatch, 1)]
     for i in range(2, outer):
-        steps += [(dispatch, i), (pair, i - 2)]
-    steps += [(pair, outer - 2), (expert, 0, 1)]
+        steps += [(pair, i - 2), (dispatch, i)]
+    steps += [(pair, i) for i in range(max(0, outer - 2), 2)]
+    steps += [(expert, 0, 1)]
     for i in range(2, outer):
+        steps += [(pair, i)] if i >= outer - 2 else []
         steps += [(give_back, 1), (give_back, 0)] if i == 2 else [(give_back, i - 1)]
-        steps += [(pair, outer - 1)] if i == outer - 1 else []
         steps += [(expert, i)]
-    steps += [(give_back, outer - 1)]
-    steps += [(combine, i) for i in range(1, outer)]
+    steps += [(combine, 1), (give_back, outer - 1)]
+    steps += [(combine, i) for i in range(2, outer)]
     return steps
 
 

time: 33.9 us -> 31.6 us (0.932)
  Pallas kernels: 33.1 us -> 30.8 us
    pallas_call x1, Pallas kernels: 33.1 us -> 30.8 us  [body(): pl.pallas_call(functools.partial(kernel, outer, inner, cap, info_width, s...]
where the time goes in v2:
time: 31.6 us; the launch traced here: 31.4 us
  Pallas kernels  30.8 us (97%)
  local copies, waits for them, and re-layouts  0.63 us (2%)
    pallas_call x1, Pallas kernels, body(): pl.pallas_call(functools.partial(kernel, outer, inner, cap, info_width, s...  30.8 us
    unnamed x1, local copies, waits for them, and re-layouts  0.63 us

profile of v2, /device:TPU:0, one launch (start us, length us, event | category | flops | bytes accessed | tf_op | source)
XLA Modules:
  0.0 31.4 jit_solution(7082936244123629430)
XLA Ops:
  0.0 30.8 %shard_map.109 = bf16[32,1024]{1,0:T(8,128)(2,1)S(1)} custom-call(bf16[32,2048]{1,0:T(8,128)(2,1)} %tokens_hbm.1, bf16[2048]{0:T(1024)(128)(2,1)} %in_gain_hbm.1, s32[6,32]{1,0:T(8,128)} %bitcast.2, f32[6,32]{1,0:T(8,128)} %bitcast.3, bf16[1024]{0:T(1024)(128)(2,1)} %out_gain_hbm.1, bf16[1,2048,384]{2,1,0:T(8,128)(2,1)} %gate_hbm.1, ...), custom_call_target="tpu_custom_call" | custom-call | tf_op jit(solution)/shard_map/pallas_call | solution.py:493
  30.8 0.6 %copy.13 = bf16[32,1024]{1,0:T(8,128)(2,1)} copy(bf16[32,1024]{1,0:T(8,128)(2,1)S(1)} %shard_map.109) | data formatting | bytes 131072

commit v3 on v2

--- a/solution.py
+++ b/solution.py
@@ -155,7 +155,7 @@
     def nth(i):
         if i == 0:
             return z
-        near = (i + 1) // 2 if i % 2 else -(i // 2)
+        near = -((i + 1) // 2) if i % 2 else i // 2
         far = jnp.where(z < outer - 1 - z, i - short, short - i)
         if i > 1:
             ends = i + 1 if i < outer - 1 else 2
@@ -183,7 +183,8 @@
 
     slot_rank = (lax.broadcasted_iota(jnp.int32, (slots, local_tokens), 0) % cap + 1).astype(F32)
     slot_of_lane = (lax.broadcasted_iota(jnp.int32, (local_tokens, slots), 1) % cap + 1).astype(F32)
-    peers = [lax.rem(p + e, inner) for e in range(1, inner)]
+
+    peers = [e + jnp.where(e < p, 0, 1) for e in range(inner - 1)]
 
     pl.semaphore_wait(barrier, outer + inner - 1)
 
@@ -275,7 +276,9 @@
             here = rows_in.at[j, :, :, mine]
             send(here, here, 1, pair_recv.at[j], ep, other)
 
-        def expert(*group):
+        opened = {}
+
+        def begin(*group):
             if group[0] == 0:
                 for load in loads[8:]:
                     load.wait()
@@ -287,31 +290,41 @@
             own_rows = rows_of(mine)
             gate_value = dot(own_rows, gate_w[mine, :])
             upward = dot(own_rows, up_w[mine, :])
+            opened[group] = gate_value, upward, rows_of
+
+        def finish(*group):
+            gate_value, upward, rows_of = opened[group]
             for i in group:
                 j = order[i]
                 arrive(rows_in.at[j, :, :, theirs], pair_recv.at[j])
             other_rows = rows_of(theirs)
             gate_value = gate_value + dot(other_rows, gate_w[theirs, :])
             upward = upward + dot(other_rows, up_w[theirs, :])
-            hidden = silu_product(gate_value, upward)
-
-            def store(target, columns):
-                values = dot(hidden, down_w[:, columns]).astype(BF16)
-                for n, i in enumerate(group):
-                    block = values[n * slots : (n + 1) * slots]
-                    target[order[i], :, :, columns] = block.reshape(inner, cap, columns.size)
-
+            opened[group] = silu_product(gate_value, upward)
             for n, piece in enumerate(pieces(other)):
-                store(part_out, piece)
+                store(group, part_out, piece)
                 for i in reversed(group):
                     j = order[i]
                     here = part_out.at[j, :, :, piece]
                     send(here, part_in.at[j, :, :, piece], 2, part_recv.at[j, n], ep, other)
+
+        def settle(*group):
             for piece in my_pieces:
-                store(part_own, piece)
+                store(group, part_own, piece)
+
+        def store(group, target, columns):
+            values = dot(opened[group], down_w[:, columns]).astype(BF16)
+            for n, i in enumerate(group):
+                block = values[n * slots : (n + 1) * slots]
+                target[order[i], :, :, columns] = block.reshape(inner, cap, columns.size)
 
         def give_back(i):
             j = order[i]
+            if i == outer - 1:
+                for k in [0] + list(range(2, outer)):
+                    weighed[k] = weigh(k)
+            if i == 1:
+                weighed[1] = weigh(1)
             for n, piece in enumerate(my_pieces):
                 arrive(part_in.at[j, :, :, piece], part_recv.at[j, n])
                 total = part_own[j, :, :, piece].astype(F32) + part_in[j, :, :, piece].astype(F32)
@@ -327,6 +340,8 @@
                     )
                 back[j, p, :, piece] = result[j, p, :, piece]
 
+        weighed = {}
+
         def weigh(i):
             known = column[order[i], :, facts_at]
             chosen = dot_t(known, pick_place) == slot_of_lane
@@ -342,9 +357,15 @@
 
         def combine(i):
             j = order[i]
-            weights = weigh(i)
+            weights = weighed.pop(i)
             for n, piece in enumerate(my_pieces):
                 sum_out[i - 1, :, piece] = gathered(i, weights, n, piece).astype(BF16)
+                if i == outer - 1 and n == 0:
+
+                    @pl.when(z == outer - 1)
+                    def _():
+                        pl.delay(DELAY)
+
                 here = sum_out.at[i - 1, :, piece]
                 send(here, sum_in.at[z, :, piece], 4, sum_recv.at[z, n], j * inner + p, core)
 
@@ -362,12 +383,12 @@
             with jax.named_scope(task.__name__ + "".join(str(w) for w in what)):
                 task(*what)
 
-        for task, *what in PLAN(outer, dispatch, shared, pair, expert, give_back, combine):
+        for task, *what in PLAN(outer, dispatch, shared, pair, begin, finish, settle, give_back, combine):
             step(task, *what)
 
         totals = []
         with jax.named_scope("own"):
-            weights = weigh(0)
+            weights = weighed[0]
             arrive(shared_in.at[:, mine], core_sem.at[0])
             for n, piece in enumerate(my_pieces):
                 shared_rows = shared_out[:, piece].astype(F32) + shared_in[:, piece].astype(F32)
@@ -433,16 +454,19 @@
             on_core(core)
 
 
-def plan(outer, dispatch, shared, pair, expert, give_back, combine):
+def plan(outer, dispatch, shared, pair, begin, finish, settle, give_back, combine):
     steps = [(dispatch, 0), (shared,), (dispatch, 1)]
     for i in range(2, outer):
         steps += [(pair, i - 2), (dispatch, i)]
     steps += [(pair, i) for i in range(max(0, outer - 2), 2)]
-    steps += [(expert, 0, 1)]
+    steps += [(begin, 0, 1), (finish, 0, 1), (settle, 0, 1)]
+    steps += [(pair, 2)] if 2 >= outer - 2 and outer > 2 else []
     for i in range(2, outer):
-        steps += [(pair, i)] if i >= outer - 2 else []
+        steps += [(begin, i)]
         steps += [(give_back, 1), (give_back, 0)] if i == 2 else [(give_back, i - 1)]
-        steps += [(expert, i)]
+        steps += [(finish, i)]
+        steps += [(pair, i + 1)] if outer - 2 <= i + 1 < outer else []
+        steps += [(settle, i)]
     steps += [(combine, 1), (give_back, outer - 1)]
     steps += [(combine, i) for i in range(2, outer)]
     return steps
@@ -452,6 +476,7 @@
 PIECES = (1, 2)
 SPLIT = 4
 RELAY = True
+DELAY = 1300
 
 
 def body(

time: 31.6 us -> 29.3 us (0.927); the launches traced: 31.4 us -> 28.8 us
  Pallas kernels: 30.8 us -> 28.1 us
    pallas_call x1, Pallas kernels: 30.8 us -> 28.1 us  [body(): pl.pallas_call(functools.partial(kernel, outer, inner, cap, info_width, s...]
where the time goes in v3:
time: 29.3 us; the launch traced here: 28.8 us
  Pallas kernels  28.1 us (96%)
  local copies, waits for them, and re-layouts  0.63 us (2%)
    pallas_call x1, Pallas kernels, body(): pl.pallas_call(functools.partial(kernel, outer, inner, cap, info_width, s...  28.1 us
    unnamed x1, local copies, waits for them, and re-layouts  0.63 us

profile of v3, /device:TPU:0, one launch (start us, length us, event | category | flops | bytes accessed | tf_op | source)
XLA Modules:
  0.0 28.8 jit_solution(4965289212110015437)
XLA Ops:
  0.0 28.1 %shard_map.109 = bf16[32,1024]{1,0:T(8,128)(2,1)S(1)} custom-call(bf16[32,2048]{1,0:T(8,128)(2,1)} %tokens_hbm.1, bf16[2048]{0:T(1024)(128)(2,1)} %in_gain_hbm.1, s32[6,32]{1,0:T(8,128)} %bitcast.2, f32[6,32]{1,0:T(8,128)} %bitcast.3, bf16[1024]{0:T(1024)(128)(2,1)} %out_gain_hbm.1, bf16[1,2048,384]{2,1,0:T(8,128)(2,1)} %gate_hbm.1, ...), custom_call_target="tpu_custom_call" | custom-call | tf_op jit(solution)/shard_map/pallas_call | solution.py:518
  28.1 0.6 %copy.13 = bf16[32,1024]{1,0:T(8,128)(2,1)} copy(bf16[32,1024]{1,0:T(8,128)(2,1)S(1)} %shard_map.109) | data formatting | bytes 131072

commit v4 on v3

--- a/solution.py
+++ b/solution.py
@@ -186,7 +186,6 @@
 
     peers = [e + jnp.where(e < p, 0, 1) for e in range(inner - 1)]
 
-    pl.semaphore_wait(barrier, outer + inner - 1)
 
     def on_core(core):
         edges = (0, split, width)
@@ -195,17 +194,19 @@
         other = 1 - core
         mine = pl.ds(first, count)
         theirs = pl.ds(edges[other], edges[other + 1] - edges[other])
+        kept = pl.ds(core * half, half)
+        given = pl.ds(other * half, half)
         facts_at = pl.ds(first, info_width)
         rows_at = pl.ds(first + info_width, count)
         sent_at = pl.ds(first, info_width + count)
 
         def pieces(which):
-            begin, stop = edges[which], edges[which + 1]
-            parts = PIECES[which] if (stop - begin) % (128 * PIECES[which]) == 0 else 1
-            size = (stop - begin) // parts
-            return [pl.ds(begin + n * size, size) for n in range(parts)]
+            if which == 0:
+                return [pl.ds(0, split)]
+            return [pl.ds(split, half - split), pl.ds(half, half)]
 
         my_pieces = pieces(core)
+        pl.semaphore_wait(barrier, outer + inner - 1)
 
         column[z, :, facts_at] = info
         column[z, :, rows_at] = rows[:, first:end]
@@ -300,6 +301,8 @@
             other_rows = rows_of(theirs)
             gate_value = gate_value + dot(other_rows, gate_w[theirs, :])
             upward = upward + dot(other_rows, up_w[theirs, :])
+            if len(group) == 1 and outer - 2 <= group[0] + 1 < outer:
+                pair(group[0] + 1)
             opened[group] = silu_product(gate_value, upward)
             for n, piece in enumerate(pieces(other)):
                 store(group, part_out, piece)
@@ -347,13 +350,14 @@
             chosen = dot_t(known, pick_place) == slot_of_lane
             high_part = jnp.where(chosen, dot_t(known, pick_high), 0.0).astype(BF16)
             low_part = jnp.where(chosen, dot_t(known, pick_low), 0.0).astype(BF16)
-            return high_part, low_part
+            return jnp.concatenate([high_part, low_part], axis=0)
 
         def gathered(i, weights, n, piece):
             j = order[i]
             arrive(back.at[j, pl.ds(0, inner - 1), :, piece], back_recv.at[j, n])
             values = back[j, :, :, piece].reshape(slots, piece.size)
-            return dot(weights[0], values) + dot(weights[1], values)
+            both = dot(weights, values)
+            return both[:local_tokens] + both[local_tokens:]
 
         def combine(i):
             j = order[i]
@@ -362,69 +366,66 @@
                 sum_out[i - 1, :, piece] = gathered(i, weights, n, piece).astype(BF16)
                 if i == outer - 1 and n == 0:
 
-                    @pl.when(z == outer - 1)
-                    def _():
-                        pl.delay(DELAY)
+                    for end, cycles in ((0, DELAY[0]), (outer - 1, DELAY[1])):
+
+                        @pl.when(z == end)
+                        def _(cycles=cycles):
+                            pl.delay(cycles)
 
                 here = sum_out.at[i - 1, :, piece]
-                send(here, sum_in.at[z, :, piece], 4, sum_recv.at[z, n], j * inner + p, core)
+                lower = core - core * n
+                send(here, sum_in.at[z, :, piece], 4, sum_recv.at[z, lower], j * inner + p, core * n)
 
         def shared():
             for load in loads[5:8]:
                 load.wait()
             inputs = normed[...]
             hidden = silu_product(dot(inputs, sgate_w[...]), dot(inputs, sup_w[...]))
-            shared_out[:, theirs] = dot(hidden, sdown_w[:, theirs]).astype(BF16)
-            here = shared_out.at[:, theirs]
-            send(here, shared_in.at[:, theirs], 5, core_sem.at[0], ep, other)
-            shared_out[:, mine] = dot(hidden, sdown_w[:, mine]).astype(BF16)
+            shared_out[:, given] = dot(hidden, sdown_w[:, given]).astype(BF16)
+            here = shared_out.at[:, given]
+            send(here, shared_in.at[:, given], 5, core_sem.at[0], ep, other)
+            shared_out[:, kept] = dot(hidden, sdown_w[:, kept]).astype(BF16)
 
         def step(task, *what):
             with jax.named_scope(task.__name__ + "".join(str(w) for w in what)):
                 task(*what)
 
-        for task, *what in PLAN(outer, dispatch, shared, pair, begin, finish, settle, give_back, combine):
+        for task, *what in PLAN(core, outer, dispatch, shared, pair, begin, finish, settle, give_back, combine):
             step(task, *what)
 
-        totals = []
         with jax.named_scope("own"):
             weights = weighed[0]
-            arrive(shared_in.at[:, mine], core_sem.at[0])
-            for n, piece in enumerate(my_pieces):
-                shared_rows = shared_out[:, piece].astype(F32) + shared_in[:, piece].astype(F32)
-                totals.append(gathered(0, weights, n, piece) + shared_rows.astype(BF16).astype(F32))
+            mixed_rows = [gathered(0, weights, n, piece) for n, piece in enumerate(my_pieces)]
+            lent = pl.ds(split, half - split)
+            if core == 1:
+                sum_out[outer - 1, :, lent] = mixed_rows[0].astype(BF16)
+                here = sum_out.at[outer - 1, :, lent]
+                send(here, sum_in.at[z, :, lent], 7, sum_recv.at[z, 1], ep, 0)
+            owned = [(my_pieces[core], 0)]
+            arrive(shared_in.at[:, kept], core_sem.at[0])
+            shared_rows = shared_out[:, kept].astype(F32) + shared_in[:, kept].astype(F32)
+            shared_rows = shared_rows.astype(BF16).astype(F32)
+            totals = [mixed_rows[core] + shared_rows[:, : my_pieces[core].size]]
+            if core == 0:
+                arrive(sum_in.at[z, :, lent], sum_recv.at[z, 1])
+                totals.append(shared_rows[:, split:] + sum_in[z, :, lent].astype(F32))
+                owned.append((lent, 1))
         with jax.named_scope("sums"):
             for i in range(1, outer):
                 j = order[i]
-                for n, piece in enumerate(my_pieces):
+                for k, (piece, n) in enumerate(owned):
                     arrive(sum_in.at[j, :, piece], sum_recv.at[j, n])
-                    totals[n] = totals[n] + sum_in[j, :, piece].astype(F32)
+                    totals[k] = totals[k] + sum_in[j, :, piece].astype(F32)
         combined = totals[0] if len(totals) == 1 else jnp.concatenate(totals, axis=1)
 
-        lanes = last_out.shape[1] - (half - split)
-        squares_at = pl.ds(half - split, lanes)
         own_squares = jnp.sum(combined * combined, axis=1, keepdims=True)
-        last_out[:, squares_at] = jnp.broadcast_to(own_squares, (local_tokens, lanes))
-        if core == 0:
-            leaving, coming = squares_at, pl.ds(0, half - split + lanes)
-        else:
-            leaving, coming = pl.ds(0, half - split + lanes), squares_at
-            if half > split:
-                last_out[:, : half - split] = combined[:, : half - split]
-        here = last_out.at[:, leaving]
-        send(here, last_in.at[:, leaving], 6, core_sem.at[1], ep, other)
+        last_out[...] = jnp.broadcast_to(own_squares, last_out.shape)
+        send(last_out, last_in, 6, core_sem.at[1], ep, other)
+        scaled = combined * out_gain[...].astype(F32)[None, :]
         with jax.named_scope("lastwait"):
-            arrive(last_in.at[:, coming], core_sem.at[1])
-        squares = own_squares + last_in[:, half - split : half - split + 1]
-        scale = lax.rsqrt(squares / width + EPSILON)
-        gain = out_gain[...].astype(F32)[None, :]
-        if core == 0:
-            mixed[:, :split] = (combined * scale * gain[:, :split]).astype(BF16)
-            if half > split:
-                extra = last_in[:, : half - split] * scale * gain[:, split:]
-                mixed[:, split:] = extra.astype(BF16)
-        else:
-            mixed[...] = (combined[:, half - split :] * scale * gain).astype(BF16)
+            arrive(last_in, core_sem.at[1])
+        squares = own_squares + last_in[:, :1]
+        mixed[...] = (scaled * lax.rsqrt(squares / width + EPSILON)).astype(BF16)
 
         for to in order[1:]:
 
@@ -443,9 +444,11 @@
         sent(rows_in.at[:, :, :, mine], 1)
         sent(part_out.at[:, :, :, theirs], 2)
         sent(result.at[:, pl.ds(0, inner - 1), :, mine], 3)
-        sent(sum_out.at[:, :, mine], 4)
-        sent(shared_out.at[:, theirs], 5)
-        sent(here, 6)
+        sent(sum_out.at[pl.ds(0, outer - 1), :, mine], 4)
+        sent(shared_out.at[:, given], 5)
+        sent(last_out, 6)
+        if core == 1:
+            sent(sum_out.at[outer - 1, :, lent], 7)
 
     for core in range(2):
 
@@ -454,7 +457,7 @@
             on_core(core)
 
 
-def plan(outer, dispatch, shared, pair, begin, finish, settle, give_back, combine):
+def plan(core, outer, dispatch, shared, pair, begin, finish, settle, give_back, combine):
     steps = [(dispatch, 0), (shared,), (dispatch, 1)]
     for i in range(2, outer):
         steps += [(pair, i - 2), (dispatch, i)]
@@ -462,21 +465,19 @@
     steps += [(begin, 0, 1), (finish, 0, 1), (settle, 0, 1)]
     steps += [(pair, 2)] if 2 >= outer - 2 and outer > 2 else []
     for i in range(2, outer):
+        earlier = [(give_back, 1), (give_back, 0)] if i == 2 else [(give_back, i - 1)]
         steps += [(begin, i)]
-        steps += [(give_back, 1), (give_back, 0)] if i == 2 else [(give_back, i - 1)]
-        steps += [(finish, i)]
-        steps += [(pair, i + 1)] if outer - 2 <= i + 1 < outer else []
+        steps += [(finish, i)] + earlier if core and i > 2 else earlier + [(finish, i)]
         steps += [(settle, i)]
-    steps += [(combine, 1), (give_back, outer - 1)]
-    steps += [(combine, i) for i in range(2, outer)]
+    steps += [(give_back, outer - 1)]
+    steps += [(combine, i) for i in range(1, outer)]
     return steps
 
 
 PLAN = plan
-PIECES = (1, 2)
-SPLIT = 4
+SPLIT = 2
 RELAY = True
-DELAY = 1300
+DELAY = (0, 1300)
 
 
 def body(
@@ -511,7 +512,7 @@
         return pltpu.VMEM(shape, kind)
 
     grid_rows = (outer, inner, cap, width)
-    most = max(PIECES)
+    most = 2
     dma = pltpu.SemaphoreType.DMA
     in_vmem = pl.BlockSpec(memory_space=pltpu.VMEM)
     in_hbm = pl.BlockSpec(memory_space=pltpu.HBM)
@@ -541,12 +542,12 @@
             vm(grid_rows),
             vm(grid_rows),
             vm(grid_rows),
-            vm((outer - 1, local_tokens, width)),
+            vm((outer, local_tokens, width)),
             vm((outer, local_tokens, width)),
             vm((local_tokens, width)),
             vm((local_tokens, width)),
-            vm((local_tokens, half - split + 128), F32),
-            vm((local_tokens, half - split + 128), F32),
+            vm((local_tokens, 128), F32),
+            vm((local_tokens, 128), F32),
             dma((11,)),
             dma((outer,)),
             dma((outer,)),
@@ -556,7 +557,7 @@
             dma((outer, most)),
             dma((outer, most)),
             dma((outer, most)),
-            dma((7,)),
+            dma((8,)),
             dma((2,)),
         ],
         compiler_params=pltpu.CompilerParams(

time: 29.3 us -> 28.8 us (0.983); the launches traced: 28.8 us -> 28.7 us
  no operation moved by 1% of the time
where the time goes in v4:
time: 28.8 us; the launch traced here: 28.7 us
  Pallas kernels  28 us (97%)
  local copies, waits for them, and re-layouts  0.63 us (2%)
    pallas_call x1, Pallas kernels, body(): pl.pallas_call(functools.partial(kernel, outer, inner, cap, info_width, s...  28 us
    unnamed x1, local copies, waits for them, and re-layouts  0.63 us

profile of v4, /device:TPU:0, one launch (start us, length us, event | category | flops | bytes accessed | tf_op | source)
XLA Modules:
  0.0 28.7 jit_solution(14687426383108576812)
XLA Ops:
  0.0 28.0 %shard_map.109 = bf16[32,1024]{1,0:T(8,128)(2,1)S(1)} custom-call(bf16[32,2048]{1,0:T(8,128)(2,1)} %tokens_hbm.1, bf16[2048]{0:T(1024)(128)(2,1)} %in_gain_hbm.1, s32[6,32]{1,0:T(8,128)} %bitcast.2, f32[6,32]{1,0:T(8,128)} %bitcast.3, bf16[1024]{0:T(1024)(128)(2,1)} %out_gain_hbm.1, bf16[1,2048,384]{2,1,0:T(8,128)(2,1)} %gate_hbm.1, ...), custom_call_target="tpu_custom_call" | custom-call | tf_op jit(solution)/shard_map/pallas_call | solution.py:519
  28.1 0.6 %copy.13 = bf16[32,1024]{1,0:T(8,128)(2,1)} copy(bf16[32,1024]{1,0:T(8,128)(2,1)S(1)} %shard_map.109) | data formatting | bytes 131072

commit v5 on v4

--- a/solution.py
+++ b/solution.py
@@ -24,13 +24,21 @@
     return (gate_value * (1.0 / (1.0 + jnp.exp(-gate_value))) * upward).astype(BF16)
 
 
+def column_sends(outer):
+    counts = []
+    for z in range(outer):
+        straight = [j for j in range(outer) if j != z and (z == 0 or abs(j - z) != 2)]
+        passed = [j for j in (z - 1, z + 1) if 0 < j < outer and 0 <= 2 * z - j < outer]
+        counts.append(len(straight) + len(passed))
+    return counts
+
+
 def kernel(
     outer,
     inner,
     cap,
     info_width,
     split,
-    relay,
     tokens_hbm,
     in_gain_hbm,
     route_expert_hbm,
@@ -70,9 +78,7 @@
     last_out,
     last_in,
     w_sem,
-    col_send,
     col_recv,
-    col_pass,
     plane_recv,
     pair_recv,
     part_recv,
@@ -163,15 +169,17 @@
         return z + jnp.where(i <= 2 * short, near, far)
 
     order = [nth(i) for i in range(outer)]
+    passing = list(order)
+    if outer > 3:
+        swap = z == outer - 2
+        passing[-2:] = [jnp.where(swap, order[-1], order[-2]), jnp.where(swap, order[-2], order[-1])]
 
     def direct(to):
-        if not relay:
-            return z >= 0
-        return (to - z) * (to - z) != 4
+        return (z == 0) | ((to - z) * (to - z) != 4)
 
     def passes(j):
         on = 2 * z - j
-        return on, ((j - z) * (j - z) == 1) & (on >= 0) & (on < outer)
+        return on, ((j - z) * (j - z) == 1) & (on >= 0) & (on < outer) & (j > 0)
 
     slots = inner * cap
     slot_row = lax.broadcasted_iota(jnp.int32, (slots, info_width), 0)
@@ -231,30 +239,39 @@
         def sent(ref, kind):
             remote(ref, ref, send_sem.at[kind], col_recv.at[0], ep, other).wait_send()
 
-        def column_copy(block, to, sem):
+        def column_copy(block, to):
             here = column.at[block, :, sent_at]
-            return remote(here, here, sem, col_recv.at[block], to * inner + p, core)
-
-        for to in order[1:]:
+            return remote(here, here, send_sem.at[8], col_recv.at[block], to * inner + p, core)
+
+        for i, to in enumerate(order[1:], 1):
+            to = jnp.where(z == 0, i, to)
 
             @pl.when(direct(to))
             def _(to=to):
-                column_copy(z, to, col_send.at[to]).start()
+                column_copy(z, to).start()
 
         pick_place = selector(0)
         pick_high = selector(experts)
         pick_low = selector(2 * experts)
 
-        def dispatch(i):
+        def dispatch(i, early=None):
+            if i < outer - 1 or i == 1:
+                move(i)
+            else:
+
+                @pl.when((z == outer - 2) == early)
+                def _():
+                    move(i)
+
+        def move(i):
             j = order[i]
             if i:
                 arrive(column.at[j, :, sent_at], col_recv.at[j])
-                if relay:
-                    on, wanted = passes(j)
-
-                    @pl.when(wanted)
-                    def _():
-                        column_copy(j, on, col_pass.at[j]).start()
+                on, wanted = passes(j)
+
+                @pl.when(wanted)
+                def _():
+                    column_copy(j, on).start()
 
             where = dot_t(pick_place, column[j, :, facts_at])
             onehot = jnp.where(where == slot_rank, 1.0, 0.0).astype(BF16)
@@ -272,7 +289,7 @@
             rows_in[j, p, :, mine] = staged[j, p, :, mine]
 
         def pair(i):
-            j = order[i]
+            j = passing[i]
             arrive(rows_in.at[j, pl.ds(0, inner - 1), :, mine], plane_recv.at[j])
             here = rows_in.at[j, :, :, mine]
             send(here, here, 1, pair_recv.at[j], ep, other)
@@ -285,7 +302,7 @@
                     load.wait()
 
             def rows_of(columns):
-                blocks = [rows_in[order[i], :, :, columns].reshape(slots, columns.size) for i in group]
+                blocks = [rows_in[passing[i], :, :, columns].reshape(slots, columns.size) for i in group]
                 return blocks[0] if len(blocks) == 1 else jnp.concatenate(blocks, axis=0)
 
             own_rows = rows_of(mine)
@@ -296,7 +313,7 @@
         def finish(*group):
             gate_value, upward, rows_of = opened[group]
             for i in group:
-                j = order[i]
+                j = passing[i]
                 arrive(rows_in.at[j, :, :, theirs], pair_recv.at[j])
             other_rows = rows_of(theirs)
             gate_value = gate_value + dot(other_rows, gate_w[theirs, :])
@@ -307,7 +324,7 @@
             for n, piece in enumerate(pieces(other)):
                 store(group, part_out, piece)
                 for i in reversed(group):
-                    j = order[i]
+                    j = passing[i]
                     here = part_out.at[j, :, :, piece]
                     send(here, part_in.at[j, :, :, piece], 2, part_recv.at[j, n], ep, other)
 
@@ -319,10 +336,10 @@
             values = dot(opened[group], down_w[:, columns]).astype(BF16)
             for n, i in enumerate(group):
                 block = values[n * slots : (n + 1) * slots]
-                target[order[i], :, :, columns] = block.reshape(inner, cap, columns.size)
+                target[passing[i], :, :, columns] = block.reshape(inner, cap, columns.size)
 
         def give_back(i):
-            j = order[i]
+            j = passing[i]
             if i == outer - 1:
                 for k in [0] + list(range(2, outer)):
                     weighed[k] = weigh(k)
@@ -346,21 +363,21 @@
         weighed = {}
 
         def weigh(i):
-            known = column[order[i], :, facts_at]
+            known = column[passing[i], :, facts_at]
             chosen = dot_t(known, pick_place) == slot_of_lane
             high_part = jnp.where(chosen, dot_t(known, pick_high), 0.0).astype(BF16)
             low_part = jnp.where(chosen, dot_t(known, pick_low), 0.0).astype(BF16)
             return jnp.concatenate([high_part, low_part], axis=0)
 
         def gathered(i, weights, n, piece):
-            j = order[i]
+            j = passing[i]
             arrive(back.at[j, pl.ds(0, inner - 1), :, piece], back_recv.at[j, n])
             values = back[j, :, :, piece].reshape(slots, piece.size)
             both = dot(weights, values)
             return both[:local_tokens] + both[local_tokens:]
 
         def combine(i):
-            j = order[i]
+            j = passing[i]
             weights = weighed.pop(i)
             for n, piece in enumerate(my_pieces):
                 sum_out[i - 1, :, piece] = gathered(i, weights, n, piece).astype(BF16)
@@ -412,7 +429,7 @@
                 owned.append((lent, 1))
         with jax.named_scope("sums"):
             for i in range(1, outer):
-                j = order[i]
+                j = passing[i]
                 for k, (piece, n) in enumerate(owned):
                     arrive(sum_in.at[j, :, piece], sum_recv.at[j, n])
                     totals[k] = totals[k] + sum_in[j, :, piece].astype(F32)
@@ -427,18 +444,12 @@
         squares = own_squares + last_in[:, :1]
         mixed[...] = (scaled * lax.rsqrt(squares / width + EPSILON)).astype(BF16)
 
-        for to in order[1:]:
-
-            @pl.when(direct(to))
-            def _(to=to):
-                column_copy(z, to, col_send.at[to]).wait_send()
-
-            if relay:
-                on, wanted = passes(to)
-
-                @pl.when(wanted)
-                def _(to=to, on=on):
-                    column_copy(to, on, col_pass.at[to]).wait_send()
+        for copies in sorted(set(column_sends(outer))):
+            planes = [plane for plane, n in enumerate(column_sends(outer)) if n == copies]
+
+            @pl.when(functools.reduce(jnp.logical_or, [z == plane for plane in planes]))
+            def _(copies=copies):
+                sent(column.at[pl.ds(0, copies), :, sent_at], 8)
 
         sent(staged.at[:, pl.ds(0, inner - 1), :, mine], 0)
         sent(rows_in.at[:, :, :, mine], 1)
@@ -460,7 +471,8 @@
 def plan(core, outer, dispatch, shared, pair, begin, finish, settle, give_back, combine):
     steps = [(dispatch, 0), (shared,), (dispatch, 1)]
     for i in range(2, outer):
-        steps += [(pair, i - 2), (dispatch, i)]
+        steps += [(dispatch, i, True)] if i == outer - 1 else []
+        steps += [(pair, i - 2), (dispatch, i, False)]
     steps += [(pair, i) for i in range(max(0, outer - 2), 2)]
     steps += [(begin, 0, 1), (finish, 0, 1), (settle, 0, 1)]
     steps += [(pair, 2)] if 2 >= outer - 2 and outer > 2 else []
@@ -476,8 +488,7 @@
 
 PLAN = plan
 SPLIT = 2
-RELAY = True
-DELAY = (0, 1300)
+DELAY = (0, 600)
 
 
 def body(
@@ -517,7 +528,7 @@
     in_vmem = pl.BlockSpec(memory_space=pltpu.VMEM)
     in_hbm = pl.BlockSpec(memory_space=pltpu.HBM)
     return pl.pallas_call(
-        functools.partial(kernel, outer, inner, cap, info_width, split, RELAY),
+        functools.partial(kernel, outer, inner, cap, info_width, split),
         out_shape=pltpu.VMEM((local_tokens, half), BF16),
         in_specs=[in_hbm] * 11,
         out_specs=in_vmem,
@@ -552,12 +563,10 @@
             dma((outer,)),
             dma((outer,)),
             dma((outer,)),
-            dma((outer,)),
-            dma((outer,)),
             dma((outer, most)),
             dma((outer, most)),
             dma((outer, most)),
-            dma((8,)),
+            dma((9,)),
             dma((2,)),
         ],
         compiler_params=pltpu.CompilerParams(

time: 28.8 us -> 28.8 us (level)
  no operation moved by 1% of the time
where the time goes in v5:
time: 28.8 us; the launch traced here: 28.7 us
  Pallas kernels  28 us (97%)
  local copies, waits for them, and re-layouts  0.63 us (2%)
    pallas_call x1, Pallas kernels, body(): pl.pallas_call(functools.partial(kernel, outer, inner, cap, info_width, s...  28 us
    unnamed x1, local copies, waits for them, and re-layouts  0.63 us

profile of v5, /device:TPU:0, one launch (start us, length us, event | category | flops | bytes accessed | tf_op | source)
XLA Modules:
  0.0 28.7 jit_solution(4854125447946291894)
XLA Ops:
  0.0 28.0 %shard_map.109 = bf16[32,1024]{1,0:T(8,128)(2,1)S(1)} custom-call(bf16[32,2048]{1,0:T(8,128)(2,1)} %tokens_hbm.1, bf16[2048]{0:T(1024)(128)(2,1)} %in_gain_hbm.1, s32[6,32]{1,0:T(8,128)} %bitcast.2, f32[6,32]{1,0:T(8,128)} %bitcast.3, bf16[1024]{0:T(1024)(128)(2,1)} %out_gain_hbm.1, bf16[1,2048,384]{2,1,0:T(8,128)(2,1)} %gate_hbm.1, ...), custom_call_target="tpu_custom_call" | custom-call | tf_op jit(solution)/shard_map/pallas_call | solution.py:530
  28.0 0.6 %copy.13 = bf16[32,1024]{1,0:T(8,128)(2,1)} copy(bf16[32,1024]{1,0:T(8,128)(2,1)S(1)} %shard_map.109) | data formatting | bytes 131072
